TPU v7x, 32 devices: a whole 2x2x4 slice. The times are simulated.
32 devices in a mesh: fs: 8 (over z, core), tp: 4 (over y, x).
Axes of the slice: x: 2, y: 2, z: 4, core: 2. Of those that a mesh axis runs over, the one named last changes fastest.
Arguments:
- saved_input: bfloat16 [6144, 2048], P('fs'), may hold values from -6 to 6
- query_cot: bfloat16 [6144, 2048], P('fs', 'tp'), may hold values from -120 to 120
- head_out: bfloat16 [6144, 2048], P('fs', 'tp'), may hold values from -120 to 120
- output_cot: bfloat16 [6144, 2048], P('fs'), may hold values from -6 to 6
- basis_q: bfloat16 [2048, 128], replicated, may hold values from -0.125 to 0.125
- basis_o: bfloat16 [2048, 128], replicated, may hold values from -0.125 to 0.125
- weight_q: float32 [2048, 2048], P('fs', 'tp'), may hold values from -0.125 to 0.125
- weight_o: float32 [2048, 2048], P('tp', 'fs'), may hold values from -0.125 to 0.125
- first_q: float32 [128, 2048], P(None, 'tp'), may hold values from -2 to 2
- second_q: float32 [128, 2048], P(None, 'tp'), may hold values from 0.01 to 1
- first_o: float32 [2048, 128], P('tp'), may hold values from -2 to 2
- second_o: float32 [2048, 128], P('tp'), may hold values from 0.01 to 1
Outputs:
- step_q: float32 [2048, 2048], P('fs', 'tp')
- step_o: float32 [2048, 2048], P('tp', 'fs')
- new_weight_q: float32 [2048, 2048], P('fs', 'tp')
- new_weight_o: float32 [2048, 2048], P('tp', 'fs')
- copy_q: bfloat16 [2048, 2048], P(None, 'tp')
- copy_o: bfloat16 [2048, 2048], P('tp')
- moment_q: float32 [128, 2048], P(None, 'tp')
- square_q: float32 [128, 2048], P(None, 'tp')
- moment_o: float32 [2048, 128], P('tp')
- square_o: float32 [2048, 128], P('tp')
All inputs are finite; a program needn't handle non-finite values.
Results may differ from a plain program's by a relative error of at most 0.0035.
Values may be sent and summed in bfloat16 or wider, within the bound.
A program may use at most 64 MiB of HBM per device.

v0:
```python
import jax
import jax.numpy as jnp
from jax import lax
from jax.sharding import PartitionSpec as P

HEADS = 16
HEAD = 128
RANK = 128
BETA_FIRST = 0.9
BETA_SECOND = 0.95
ADAM_EPS = 1e-08
NORM_EPS = 1e-06
CLIP_RMS = 1.0
LEARN_RATE = 0.01


def split_product(factor_part, data_part):
    upper = factor_part.astype(jnp.bfloat16)
    lower = (factor_part - upper.astype(jnp.float32)).astype(jnp.bfloat16)
    first = jnp.dot(upper, data_part, preferred_element_type=jnp.float32)
    return first + jnp.dot(lower, data_part, preferred_element_type=jnp.float32)


def shards(
    saved_input,
    query_cot,
    head_out,
    output_cot,
    basis_q,
    basis_o,
    weight_q,
    weight_o,
    first_q,
    second_q,
    first_o,
    second_o,
):
    highest = lax.Precision.HIGHEST
    row_count = weight_q.shape[0]
    offset = lax.axis_index("fs") * row_count
    rows_q = lax.dynamic_slice_in_dim(basis_q, offset, row_count, 0).astype(jnp.float32)
    rows_o = lax.dynamic_slice_in_dim(basis_o, offset, row_count, 0).astype(jnp.float32)
    input_low = jnp.dot(saved_input, basis_q, preferred_element_type=jnp.float32)
    partial_q = split_product(input_low.T, query_cot)
    cot_low = jnp.dot(output_cot, basis_o, preferred_element_type=jnp.float32)
    partial_o = split_product(cot_low.T, head_out).T
    low_q, low_o = lax.psum((partial_q, partial_o), "fs")
    sum_q, sum_o = lax.psum((jnp.sum(low_q * low_q), jnp.sum(low_o * low_o)), "tp")
    rms_value = jnp.sqrt((sum_q + sum_o) / (2 * RANK * HEADS * HEAD) + NORM_EPS)
    factor = jnp.minimum(1.0, CLIP_RMS / rms_value)
    moment_q = BETA_FIRST * first_q + (1.0 - BETA_FIRST) * factor * low_q
    square_q = BETA_SECOND * second_q + (1.0 - BETA_SECOND) * (factor * low_q) ** 2
    moment_o = BETA_FIRST * first_o + (1.0 - BETA_FIRST) * factor * low_o
    square_o = BETA_SECOND * second_o + (1.0 - BETA_SECOND) * (factor * low_o) ** 2
    dir_q = moment_q / (jnp.sqrt(square_q) + ADAM_EPS)
    dir_o = moment_o / (jnp.sqrt(square_o) + ADAM_EPS)
    step_q = jnp.dot(rows_q, dir_q, precision=highest)
    step_o = jnp.dot(dir_o, rows_o.T, precision=highest)
    new_weight_q = weight_q - LEARN_RATE * step_q
    new_weight_o = weight_o - LEARN_RATE * step_o
    copy_q, copy_o = (
        lax.all_gather(new_weight_q.astype(jnp.bfloat16), "fs", axis=0, tiled=True),
        lax.all_gather(new_weight_o.astype(jnp.bfloat16), "fs", axis=1, tiled=True),
    )
    return (
        step_q,
        step_o,
        new_weight_q,
        new_weight_o,
        copy_q,
        copy_o,
        moment_q,
        square_q,
        moment_o,
        square_o,
    )


def solution(mesh):
    return jax.shard_map(
        shards,
        mesh=mesh,
        in_specs=(
            P("fs", None),
            P("fs", "tp"),
            P("fs", "tp"),
            P("fs", None),
            P(),
            P(),
            P("fs", "tp"),
            P("tp", "fs"),
            P(None, "tp"),
            P(None, "tp"),
            P("tp", None),
            P("tp", None),
        ),
        out_specs=(
            P("fs", "tp"),
            P("tp", "fs"),
            P("fs", "tp"),
            P("tp", "fs"),
            P(None, "tp"),
            P("tp", None),
            P(None, "tp"),
            P(None, "tp"),
            P("tp", None),
            P("tp", None),
        ),
        check_vma=False,
    )
```

profile of v0, /device:TPU:0, one launch (start us, length us, event | category | flops | bytes accessed | tf_op | source)
XLA Modules:
  0.0 164.3 jit_solution(583530073985837648)
XLA Ops:
  7.2 0.0 copy-start
  7.2 0.0 all-reduce.3.cloned.1.call-start
  7.2 1.8 %copy-done = bf16[768,2048]{1,0:T(8,128)(2,1)S(1)} copy-done((bf16[768,2048]{1,0:T(8,128)(2,1)S(1)}, bf16[768,2048]{1,0:T(8,128)(2,1)}, u32[]{:S(2)}) %copy-start) | copy-done | bytes 3145752
  9.1 0.0 copy-start.2
  9.1 0.0 copy-start.1
  9.1 0.0 copy-start.8
  9.1 2.4 %fusion.25 = f32[128,768]{1,0:T(8,128)S(1)} fusion(bf16[2048,128]{1,0:T(8,128)(2,1)} %param.16, bf16[768,2048]{1,0:T(8,128)(2,1)S(1)} %copy-done), kind=kOutput, calls=%fused_computation.37 | convolution fusion | flops 402653184 | bytes 4063232 | tf_op jit(solution)/shard_map/dot_general | solution.py:43
  11.4 0.0 copy-done.2
  11.5 0.3 fusion.15
  11.7 0.0 copy-start.3
  11.7 1.0 convolution_add_fusion.1
  12.7 0.0 copy-done.1
  12.7 0.0 copy-done.8
  12.7 0.0 copy-start.9
  12.7 1.2 fusion.26
  13.9 0.0 copy-done.3
  13.9 0.3 fusion.12
  14.2 1.0 fusion
  15.2 0.0 all-reduce.3.cloned.1.call-update
  15.2 0.0 all-gather.5.cloned.1.call-start
  15.2 0.0 copy-done.9
  15.2 0.8 copy.22
  16.1 1.8 %copy.23 = f32[512,128]{0,1:T(8,128)} copy(f32[512,128]{1,0:T(8,128)} %param.23) | data formatting | bytes 524288 | tf_op args[11]
  17.9 56.8 %all-reduce.3.cloned.1.call-done = (f32[128,512]{1,0:T(8,128)}, f32[512,128]{0,1:T(8,128)}) async-done(((f32[128,512]{1,0:T(8,128)}, f32[512,128]{0,1:T(8,128)}), (f32[128,512]{1,0:T(8,128)}, f32[512,128]{0,1:T(8,128)})) %all-reduce.3.cloned.1.call-update) | async-done | bytes 524304 | tf_op jit(solution)/shard_map/psum | solution.py:47
  74.7 1.6 multiply_reduce_fusion
  76.3 1.6 multiply_reduce_fusion.1
  79.2 10.3 %psum.32 = f32[]{:T(128)} all-reduce(f32[]{:T(128)S(6)} %add.56), channel_id=1, replica_groups=mesh['fs'=8,'tp'=4] {'tp'}, use_global_device_ids=true, to_apply=%region_2.0 | all-reduce | flops 1 | bytes 8 | tf_op jit(solution)/shard_map/psum | solution.py:48
  90.3 1.2 multiply_add_fusion
  91.5 0.0 copy-start.4
  91.5 0.7 copy-done.4
  92.2 2.6 %fusion.23 = (bf16[512,256]{1,0:T(8,128)(2,1)}, f32[512,256]{1,0:T(8,128)}, f32[512,256]{1,0:T(8,128)}) fusion(f32[512,256]{1,0:T(8,128)} %param.19, bf16[2048,128]{1,0:T(8,128)(2,1)} %param.17, s32[]{:T(128)S(6)} %select_n.4, f32[512,128]{0,1:T(8,128)S(1)} %get-tuple-element.27, f32[512,128]{0,1:T(8,128)S(1)} %get-tuple-element.26), kind=kOutput, calls=%fused_computation.35 | convolution fusion | flops 201850880 | bytes 2424836 | tf_op jit(solution)/shard_map/dot_general | solution.py:58
  94.8 0.0 all-gather.5.cloned.1.call-update
  94.8 0.0 all-gather.3.cloned.1.call-start
  94.9 1.2 multiply_add_fusion.2
  96.1 0.0 copy-start.6
  96.1 0.0 copy-start.7
  96.1 0.7 copy-done.6
  96.8 2.6 %fusion.24 = (bf16[256,512]{1,0:T(8,128)(2,1)}, f32[256,512]{1,0:T(8,128)}, f32[256,512]{1,0:T(8,128)}) fusion(f32[256,512]{1,0:T(8,128)} %param.18, f32[128,512]{1,0:T(8,128)S(1)} %get-tuple-element.48, f32[128,512]{1,0:T(8,128)S(1)} %get-tuple-element.49, bf16[2048,128]{1,0:T(8,128)(2,1)} %param.16, s32[]{:T(128)S(6)} %select_n.4), kind=kOutput, calls=%fused_computation.36 | convolution fusion | flops 201850880 | bytes 2424836 | tf_op jit(solution)/shard_map/dot_general | solution.py:57
  99.4 0.0 copy-done.7
  99.4 0.0 all-gather.3.cloned.1.call-update
  99.4 1.8 %copy.25 = f32[512,128]{1,0:T(8,128)} copy(f32[512,128]{0,1:T(8,128)} %copy-done.4) | data formatting | bytes 524288
  101.2 0.8 copy.24
  102.1 20.8 %all-gather.5.cloned.1.call-done = bf16[512,2048]{1,0:T(8,128)(2,1)} async-done(((bf16[512,256]{1,0:T(8,128)(2,1)}), bf16[512,2048]{1,0:T(8,128)(2,1)}) %all-gather.5.cloned.1.call-update) | async-done | bytes 2097168 | tf_op jit(solution)/shard_map/all_gather | solution.py:63
  122.8 30.4 %all-gather.3.cloned.1.call-done = bf16[2048,512]{1,0:T(8,128)(2,1)} async-done(((bf16[256,512]{1,0:T(8,128)(2,1)}), bf16[2048,512]{1,0:T(8,128)(2,1)}) %all-gather.3.cloned.1.call-update) | async-done | bytes 2097168 | tf_op jit(solution)/shard_map/all_gather | solution.py:62
  153.2 0.0 copy-start.5
  153.2 3.2 %copy.30 = bf16[2048,512]{1,0:T(8,128)(2,1)} copy(bf16[2048,512]{1,0:T(8,128)(2,1)} %all-gather.3.cloned.1.call-done) | data formatting | bytes 4194304
  156.4 0.0 copy-done.5
  156.4 1.3 copy.31
Async XLA Ops:
  7.2 1.9 %copy-start = (bf16[768,2048]{1,0:T(8,128)(2,1)S(1)}, bf16[768,2048]{1,0:T(8,128)(2,1)}, u32[]{:S(2)}) copy-start(bf16[768,2048]{1,0:T(8,128)(2,1)} %param.12) | copy-start | bytes 9437188
  7.2 67.5 %all-reduce.3.cloned.1.call-start = ((), (), s32[]{:S(2)}) async-start(), calls=%async_computation.2 | async-start | bytes 1048576 | tf_op jit(solution)/shard_map/psum | solution.py:47
  9.1 2.4 %copy-start.2 = (bf16[768,512]{1,0:T(8,128)(2,1)S(1)}, bf16[768,512]{1,0:T(8,128)(2,1)}, u32[]{:S(2)}) copy-start(bf16[768,512]{1,0:T(8,128)(2,1)} %param.13) | copy-start | bytes 2359300
  9.1 3.6 %copy-start.1 = (bf16[768,2048]{1,0:T(8,128)(2,1)S(1)}, bf16[768,2048]{1,0:T(8,128)(2,1)}, u32[]{:S(2)}) copy-start(bf16[768,2048]{1,0:T(8,128)(2,1)} %param.15) | copy-start | bytes 9437188
  9.1 3.6 %copy-start.8 = (bf16[2048,128]{1,0:T(8,128)(2,1)S(1)}, bf16[2048,128]{1,0:T(8,128)(2,1)}, u32[]{:S(2)}) copy-start(bf16[2048,128]{1,0:T(8,128)(2,1)} %param.17) | copy-start | bytes 1572868
  11.7 2.2 %copy-start.3 = (bf16[768,512]{1,0:T(8,128)(2,1)S(1)}, bf16[768,512]{1,0:T(8,128)(2,1)}, u32[]{:S(2)}) copy-start(bf16[768,512]{1,0:T(8,128)(2,1)} %param.14) | copy-start | bytes 2359300
  12.7 2.5 %copy-start.9 = (f32[512,128]{1,0:T(8,128)S(1)}, f32[512,128]{1,0:T(8,128)}, u32[]{:S(2)}) copy-start(f32[512,128]{1,0:T(8,128)} %param.22) | copy-start | bytes 786436
  15.2 107.7 %all-gather.5.cloned.1.call-start = ((), (), s32[]{:S(2)}) async-start(), calls=%async_computation.1 | async-start | bytes 2359296 | tf_op jit(solution)/shard_map/all_gather | solution.py:63
  91.5 0.7 copy-start.4
  94.8 58.4 %all-gather.3.cloned.1.call-start = ((), (), s32[]{:S(2)}) async-start(), calls=%async_computation | async-start | bytes 2359296 | tf_op jit(solution)/shard_map/all_gather | solution.py:62
  96.1 0.7 copy-start.6
  96.1 3.3 %copy-start.7 = (f32[128,512]{1,0:T(8,128)}, f32[128,512]{1,0:T(8,128)S(1)}, u32[]{:S(2)}) copy-start(f32[128,512]{1,0:T(8,128)S(1)} %get-tuple-element.48) | copy-start | bytes 786436
  153.2 3.2 %copy-start.5 = (bf16[512,2048]{1,0:T(8,128)(2,1)S(1)}, bf16[512,2048]{1,0:T(8,128)(2,1)}, u32[]{:S(2)}) copy-start(bf16[512,2048]{1,0:T(8,128)(2,1)} %all-gather.5.cloned.1.call-done) | copy-start | bytes 6291460
Sparse Core Ops, SparseCore 0:
  15.3 59.3 all-reduce.2
  94.9 27.8 all-gather.4
  125.0 28.1 all-gather.2
where the time goes:
time: 165 us; the launch traced here: 164 us
  waiting for transfers between devices  108 us (65%)
  between operations  15.9 us (10%)
  local copies, waits for them, and re-layouts  13 us (8%)
  matrix products  11.2 us (7%)
  blocking collectives  10.3 us (6%)
  other arithmetic  5.64 us (3%)
    psum x1, waiting for transfers between devices, shards(): low_q, low_o = lax.psum((partial_q, partial_o), 'fs')  56.8 us
    all_gather x1, waiting for transfers between devices, shards(): lax.all_gather(new_weight_q.astype(jnp.bfloat16), 'fs', axis=0, tiled=True)  30.4 us
    all_gather x1, waiting for transfers between devices, shards(): lax.all_gather(new_weight_o.astype(jnp.bfloat16), 'fs', axis=1, tiled=True)  20.8 us
    unnamed x26, local copies, waits for them, and re-layouts  13 us
    psum x1, blocking collectives, shards(): lax.psum((jnp.sum(low_q * low_q), jnp.sum(low_o * low_o)), 'tp')  10.3 us
  transfers between devices with their start and end apart: 3, of which 3 were waited for; matrix products, arithmetic and copies ran while one was open for 6% of the time, Pallas kernels for 0%

commit v1 on v0

--- a/solution.py
+++ b/solution.py
@@ -60,7 +60,7 @@
     new_weight_o = weight_o - LEARN_RATE * step_o
     copy_q, copy_o = (
         lax.all_gather(new_weight_q.astype(jnp.bfloat16), "fs", axis=0, tiled=True),
-        lax.all_gather(new_weight_o.astype(jnp.bfloat16), "fs", axis=1, tiled=True),
+        jnp.concatenate(lax.all_gather(new_weight_o.astype(jnp.bfloat16), "fs"), axis=1),
     )
     return (
         step_q,

time: 165 us -> 162 us (0.982)
  waiting for transfers between devices: 108 us -> 104 us
  local copies, waits for them, and re-layouts: 13 us -> 14.7 us
    reshape x0 -> x1, local copies, waits for them, and re-layouts: none -> 3.19 us  [shards(): jnp.concatenate(lax.all_gather(new_weight_o.astype(jnp.bfloat16), 'fs'),...]
    all_gather x1, waiting for transfers between devices: 30.4 us -> 27.6 us  [shards(): lax.all_gather(new_weight_q.astype(jnp.bfloat16), 'fs', axis=0, tiled=True)]
    unnamed x26 -> x23, local copies, waits for them, and re-layouts: 13 us -> 11.5 us
  transfers between devices with their start and end apart: 3 -> 3, of which waited for: 3 -> 3; matrix products, arithmetic and copies ran while one was open for 6% -> 8% of each run, Pallas kernels for 0% -> 0%
where the time goes in v1:
time: 162 us
  waiting for transfers between devices  104 us (64%)
  between operations  15.9 us (10%)
  local copies, waits for them, and re-layouts  14.7 us (9%)
  matrix products  11.2 us (7%)
  blocking collectives  10.3 us (6%)
  other arithmetic  5.64 us (3%)
    psum x1, waiting for transfers between devices, shards(): low_q, low_o = lax.psum((partial_q, partial_o), 'fs')  56.8 us
    all_gather x1, waiting for transfers between devices, shards(): lax.all_gather(new_weight_q.astype(jnp.bfloat16), 'fs', axis=0, tiled=True)  27.6 us
    all_gather x1, waiting for transfers between devices, shards(): lax.all_gather(new_weight_o.astype(jnp.bfloat16), 'fs')  19.3 us
    unnamed x23, local copies, waits for them, and re-layouts  11.5 us
    psum x1, blocking collectives, shards(): lax.psum((jnp.sum(low_q * low_q), jnp.sum(low_o * low_o)), 'tp')  10.3 us
  transfers between devices with their start and end apart: 3, of which 3 were waited for; matrix products, arithmetic and copies ran while one was open for 8% of the time, Pallas kernels for 0%

profile of v1, /device:TPU:0, one launch (start us, length us, event | category | flops | bytes accessed | tf_op | source)
XLA Modules:
  0.0 161.7 jit_solution(15809549713658101379)
XLA Ops:
  7.2 0.0 copy-start
  7.2 0.0 all-reduce.3.cloned.1.call-start
  7.2 1.8 %copy-done = bf16[768,2048]{1,0:T(8,128)(2,1)S(1)} copy-done((bf16[768,2048]{1,0:T(8,128)(2,1)S(1)}, bf16[768,2048]{1,0:T(8,128)(2,1)}, u32[]{:S(2)}) %copy-start) | copy-done | bytes 3145752
  9.1 0.0 copy-start.2
  9.1 0.0 copy-start.1
  9.1 0.0 copy-start.7
  9.1 2.4 %fusion.25 = f32[128,768]{1,0:T(8,128)S(1)} fusion(bf16[2048,128]{1,0:T(8,128)(2,1)} %param.16, bf16[768,2048]{1,0:T(8,128)(2,1)S(1)} %copy-done), kind=kOutput, calls=%fused_computation.37 | convolution fusion | flops 402653184 | bytes 4063232 | tf_op jit(solution)/shard_map/dot_general | solution.py:43
  11.4 0.0 copy-done.2
  11.5 0.3 fusion.15
  11.7 0.0 copy-start.3
  11.7 1.0 convolution_add_fusion.1
  12.7 0.0 copy-done.1
  12.7 0.0 copy-done.7
  12.7 0.0 copy-start.8
  12.7 1.2 fusion.26
  13.9 0.0 copy-done.3
  13.9 0.3 fusion.12
  14.2 1.0 fusion
  15.2 0.0 all-reduce.3.cloned.1.call-update
  15.2 0.0 all-gather.6.cloned.1.call-start
  15.2 0.0 copy-done.8
  15.2 0.8 copy.22
  16.1 1.8 %copy.23 = f32[512,128]{0,1:T(8,128)} copy(f32[512,128]{1,0:T(8,128)} %param.23) | data formatting | bytes 524288 | tf_op args[11]
  17.9 56.8 %all-reduce.3.cloned.1.call-done = (f32[128,512]{1,0:T(8,128)}, f32[512,128]{0,1:T(8,128)}) async-done(((f32[128,512]{1,0:T(8,128)}, f32[512,128]{0,1:T(8,128)}), (f32[128,512]{1,0:T(8,128)}, f32[512,128]{0,1:T(8,128)})) %all-reduce.3.cloned.1.call-update) | async-done | bytes 524304 | tf_op jit(solution)/shard_map/psum | solution.py:47
  74.7 1.6 %multiply_reduce_fusion = f32[]{:T(128)} fusion(f32[512,128]{0,1:T(8,128)} %get-tuple-element.21), kind=kLoop, calls=%fused_computation.19 | loop fusion | flops 131071 | bytes 262148 | tf_op jit(solution)/shard_map/reduce_sum | solution.py:48
  76.3 1.6 %multiply_reduce_fusion.1 = f32[]{:T(128)} fusion(f32[128,512]{1,0:T(8,128)} %get-tuple-element.20), kind=kLoop, calls=%fused_computation.20 | loop fusion | flops 131071 | bytes 262148 | tf_op jit(solution)/shard_map/reduce_sum | solution.py:48
  79.2 10.3 %psum.32 = f32[]{:T(128)} all-reduce(f32[]{:T(128)S(6)} %add.56), channel_id=1, replica_groups=mesh['fs'=8,'tp'=4] {'tp'}, use_global_device_ids=true, to_apply=%region_2.0 | all-reduce | flops 1 | bytes 8 | tf_op jit(solution)/shard_map/psum | solution.py:48
  90.3 1.2 multiply_add_fusion
  91.5 0.0 copy-start.4
  91.5 0.7 copy-done.4
  92.2 2.6 %fusion.23 = (bf16[512,256]{1,0:T(8,128)(2,1)}, f32[512,256]{1,0:T(8,128)}, f32[512,256]{1,0:T(8,128)}) fusion(f32[512,256]{1,0:T(8,128)} %param.19, bf16[2048,128]{1,0:T(8,128)(2,1)} %param.17, s32[]{:T(128)S(6)} %select_n.4, f32[512,128]{0,1:T(8,128)S(1)} %get-tuple-element.27, f32[512,128]{0,1:T(8,128)S(1)} %get-tuple-element.26), kind=kOutput, calls=%fused_computation.35 | convolution fusion | flops 201850880 | bytes 2424836 | tf_op jit(solution)/shard_map/dot_general | solution.py:58
  94.8 0.0 all-gather.6.cloned.1.call-update
  94.8 0.0 all-gather.4.cloned.1.call-start
  94.9 1.2 multiply_add_fusion.2
  96.1 0.0 copy-start.5
  96.1 0.0 copy-start.6
  96.1 0.7 copy-done.5
  96.8 2.6 %fusion.24 = (bf16[256,512]{1,0:T(8,128)(2,1)}, f32[256,512]{1,0:T(8,128)}, f32[256,512]{1,0:T(8,128)}) fusion(f32[256,512]{1,0:T(8,128)} %param.18, f32[128,512]{1,0:T(8,128)S(1)} %get-tuple-element.48, f32[128,512]{1,0:T(8,128)S(1)} %get-tuple-element.49, bf16[2048,128]{1,0:T(8,128)(2,1)} %param.16, s32[]{:T(128)S(6)} %select_n.4), kind=kOutput, calls=%fused_computation.36 | convolution fusion | flops 201850880 | bytes 2424836 | tf_op jit(solution)/shard_map/dot_general | solution.py:57
  99.4 0.0 copy-done.6
  99.4 0.0 all-gather.4.cloned.1.call-update
  99.4 1.8 %copy.26 = f32[512,128]{1,0:T(8,128)} copy(f32[512,128]{0,1:T(8,128)} %copy-done.4) | data formatting | bytes 524288
  101.2 0.8 copy.25
  102.1 19.3 %all-gather.6.cloned.1.call-done = bf16[4096,256]{1,0:T(8,128)(2,1)} async-done(((bf16[512,256]{1,0:T(8,128)(2,1)}), bf16[4096,256]{1,0:T(8,128)(2,1)}) %all-gather.6.cloned.1.call-update) | async-done | bytes 2097168 | tf_op jit(solution)/shard_map/all_gather | solution.py:63
  121.4 3.2 %copy.27 = bf16[8,64,8,256]{3,2,0,1:T(8,128)(2,1)} copy(bf16[8,64,8,256]{3,2,1,0:T(8,128)(2,1)} %bitcast.15) | data formatting | bytes 4194304 | tf_op jit(solution)/shard_map/reshape | solution.py:63
  124.6 27.6 %all-gather.4.cloned.1.call-done = bf16[2048,512]{1,0:T(8,128)(2,1)} async-done(((bf16[256,512]{1,0:T(8,128)(2,1)}), bf16[2048,512]{1,0:T(8,128)(2,1)}) %all-gather.4.cloned.1.call-update) | async-done | bytes 2097168 | tf_op jit(solution)/shard_map/all_gather | solution.py:62
  152.1 3.0 %copy.31 = bf16[2048,512]{1,0:T(8,128)(2,1)} copy(bf16[2048,512]{1,0:T(8,128)(2,1)} %all-gather.4.cloned.1.call-done) | data formatting | bytes 4194304
Async XLA Ops:
  7.2 1.9 %copy-start = (bf16[768,2048]{1,0:T(8,128)(2,1)S(1)}, bf16[768,2048]{1,0:T(8,128)(2,1)}, u32[]{:S(2)}) copy-start(bf16[768,2048]{1,0:T(8,128)(2,1)} %param.12) | copy-start | bytes 9437188
  7.2 67.5 %all-reduce.3.cloned.1.call-start = ((), (), s32[]{:S(2)}) async-start(), calls=%async_computation.2 | async-start | bytes 1048576 | tf_op jit(solution)/shard_map/psum | solution.py:47
  9.1 2.4 %copy-start.2 = (bf16[768,512]{1,0:T(8,128)(2,1)S(1)}, bf16[768,512]{1,0:T(8,128)(2,1)}, u32[]{:S(2)}) copy-start(bf16[768,512]{1,0:T(8,128)(2,1)} %param.13) | copy-start | bytes 2359300
  9.1 3.6 %copy-start.1 = (bf16[768,2048]{1,0:T(8,128)(2,1)S(1)}, bf16[768,2048]{1,0:T(8,128)(2,1)}, u32[]{:S(2)}) copy-start(bf16[768,2048]{1,0:T(8,128)(2,1)} %param.15) | copy-start | bytes 9437188
  9.1 3.6 %copy-start.7 = (bf16[2048,128]{1,0:T(8,128)(2,1)S(1)}, bf16[2048,128]{1,0:T(8,128)(2,1)}, u32[]{:S(2)}) copy-start(bf16[2048,128]{1,0:T(8,128)(2,1)} %param.17) | copy-start | bytes 1572868
  11.7 2.2 %copy-start.3 = (bf16[768,512]{1,0:T(8,128)(2,1)S(1)}, bf16[768,512]{1,0:T(8,128)(2,1)}, u32[]{:S(2)}) copy-start(bf16[768,512]{1,0:T(8,128)(2,1)} %param.14) | copy-start | bytes 2359300
  12.7 2.5 %copy-start.8 = (f32[512,128]{1,0:T(8,128)S(1)}, f32[512,128]{1,0:T(8,128)}, u32[]{:S(2)}) copy-start(f32[512,128]{1,0:T(8,128)} %param.22) | copy-start | bytes 786436
  15.2 106.2 %all-gather.6.cloned.1.call-start = ((), (), s32[]{:S(2)}) async-start(), calls=%async_computation.1 | async-start | bytes 2359296 | tf_op jit(solution)/shard_map/all_gather | solution.py:63
  91.5 0.7 copy-start.4
  94.8 57.3 %all-gather.4.cloned.1.call-start = ((), (), s32[]{:S(2)}) async-start(), calls=%async_computation | async-start | bytes 2359296 | tf_op jit(solution)/shard_map/all_gather | solution.py:62
  96.1 0.7 copy-start.5
  96.1 3.3 %copy-start.6 = (f32[128,512]{1,0:T(8,128)}, f32[128,512]{1,0:T(8,128)S(1)}, u32[]{:S(2)}) copy-start(f32[128,512]{1,0:T(8,128)S(1)} %get-tuple-element.48) | copy-start | bytes 786436
Sparse Core Ops, SparseCore 0:
  15.3 59.3 all-reduce.2
  94.9 26.3 all-gather.5
  123.5 28.5 all-gather.3
